TPU v7x, 32 devices: a whole 2x2x4 slice. The times are simulated.
32 devices in a mesh: grp: 2 (over y), sp: 4 (over z), tp: 4 (over x, core).
Axes of the slice: x: 2, y: 2, z: 4, core: 2. Of those that a mesh axis runs over, the one named last changes fastest.
Arguments:
- recurrent_query: bfloat16 [2048, 1024], P(('grp', 'sp'), 'tp'), parts along dimension 0, may hold values from -6 to 6
- recurrent_forget_gate: bfloat16 [2048, 1024], P(('grp', 'sp'), 'tp'), parts along dimension 0, may hold values from -4.5 to 4.5
- recurrent_value: bfloat16 [2048, 1024], P(('grp', 'sp'), 'tp'), parts along dimension 0, may hold values from -6 to 6
- recurrent_gate_lower_bound: float32 [1024], P('tp'), may hold values from 1.5 to 14
- recurrent_added_decay: float32 [2048, 8], P(('grp', 'sp'), 'tp'), parts along dimension 0, may hold values from -0.51 to 0
- recurrent_norm_gain: float32 [128], replicated, may hold values from 0.1 to 1.9
- attention_query_first: bfloat16 [2048, 512], P(('grp', 'sp'), 'tp'), parts along dimension 0, may hold values from -20 to 20
- attention_key_first: bfloat16 [2048, 256], P(('grp', 'sp'), 'tp'), parts along dimension 0, may hold values from -20 to 20
- attention_query_second: bfloat16 [2048, 512], P(('grp', 'sp'), 'tp'), parts along dimension 0, may hold values from -20 to 20
- attention_key_second: bfloat16 [2048, 256], P(('grp', 'sp'), 'tp'), parts along dimension 0, may hold values from -20 to 20
- attention_value: bfloat16 [2048, 512], P(('grp', 'sp'), 'tp'), parts along dimension 0, may hold values from -6 to 6
- second_map_weight: float32 [8], P('tp'), may hold values from 0.3 to 0.8
- attention_norm_gain: float32 [128], replicated, may hold values from 0.1 to 1.9
- output_weight: bfloat16 [2, 1024, 2048], P(None, 'tp', 'sp'), may hold values from -0.125 to 0.125
Outputs:
- mixed: bfloat16 [2048, 2048], P(('grp', 'sp', 'tp')), parts along dimension 0
There are 2 independent parts, one for each index of `grp`. A program takes and returns all parts, laid end to end along the dimension named above; an argument that names none is the same for every part. Nothing has to cross between parts.
All inputs are finite; a program needn't handle non-finite values.
Results may differ from a plain program's by a relative error of at most 0.02.
Values may be sent and summed in bfloat16 or wider, within the bound.
A program may use at most 64 MiB of HBM per device.

v0:
```python
import jax
import jax.numpy as jnp
from jax import lax
from jax.sharding import PartitionSpec as P

HG_DK = 128
HG_DV = 128
DA_HD = 64
BLK = 32
epsilon = 1e-06
highest = lax.Precision.HIGHEST
key_span = 512


def carried_in(array, axis, combine, identity):
    size, place = (lax.axis_size(axis), lax.axis_index(axis))
    everything = jax.tree.map(
        lambda part, kind: lax.all_gather(part.astype(kind), axis),
        array,
        (jnp.bfloat16, jnp.bfloat16),
    )
    start = jax.tree.map(
        lambda part, zero: jnp.broadcast_to(jnp.asarray(zero, part.dtype), part.shape),
        array,
        identity,
    )

    def hop(k, before):
        reached = k < place
        new = combine(
            before, jax.tree.map(lambda part, own: part[k].astype(own.dtype), everything, array)
        )
        return jax.tree.map(lambda a, b: jnp.where(reached, a, b), new, before)

    return lax.fori_loop(0, size, hop, start)


def head_norm(head_values, gain_vec):
    mean_square = jnp.mean(head_values * head_values, axis=-1, keepdims=True)
    return head_values * lax.rsqrt(mean_square + epsilon) * gain_vec


def decay_factors(gate_preactivation, lower_bound_logit, added_log_decay, number_of_heads):
    token_count = gate_preactivation.shape[0]
    floor_rate = jax.nn.sigmoid(-lower_bound_logit).reshape(number_of_heads, -1)
    state_inflow = floor_rate[None] * jax.nn.sigmoid(
        -gate_preactivation.astype(jnp.float32)
    ).reshape(token_count, number_of_heads, -1)
    decay_logarithm = jnp.log1p(-state_inflow) + added_log_decay[:, :, None]
    return (state_inflow, decay_logarithm)


def recurrence_blocks(queries, decay_logarithm, state_inflow, value_rows, block_len):
    token_count, number_of_heads, key_width = queries.shape
    block_count = token_count // block_len

    def to_blocks(source):
        return source.reshape(block_count, block_len, number_of_heads, source.shape[-1])

    causal = jnp.tril(jnp.ones((block_len, block_len), jnp.float32))[:, :, None, None]

    def block_step(carry_state, inputs):
        query_blk, decay_blk, inflow_blk, value_blk = inputs
        cumulative = jnp.cumsum(decay_blk, axis=0)
        relative = cumulative[:, None] - cumulative[None, :]
        decay_table = jnp.exp(jnp.minimum(relative, 0.0)) * causal
        scores = jnp.einsum(
            "thd,shd,tshd->hts", query_blk, inflow_blk, decay_table, precision=highest
        )
        block_out = jnp.einsum("hts,shv->thv", scores, value_blk, precision=highest)
        block_out = block_out + jnp.einsum(
            "thd,hdv->thv", query_blk * jnp.exp(cumulative), carry_state, precision=highest
        )
        last_log = cumulative[-1]
        new_state = jnp.exp(last_log)[:, :, None] * carry_state + jnp.einsum(
            "shd,shv->hdv",
            inflow_blk * jnp.exp(last_log[None] - cumulative),
            value_blk,
            precision=highest,
        )
        return (new_state, block_out)

    zero_state = jnp.zeros((number_of_heads, key_width, value_rows.shape[-1]), jnp.float32)
    final_state, outputs = lax.scan(
        block_step,
        zero_state,
        (
            to_blocks(queries),
            to_blocks(decay_logarithm),
            to_blocks(state_inflow),
            to_blocks(value_rows),
        ),
    )
    return (final_state, outputs.reshape(token_count, number_of_heads, -1))


def chain_pair(earlier, following):
    return (earlier[0] * following[0], following[0][:, :, None] * earlier[1] + following[1])


def recurrent_path_output(
    recurrent_query,
    recurrent_forget_gate,
    recurrent_value,
    recurrent_gate_lower_bound,
    recurrent_added_decay,
    recurrent_norm_gain,
):
    token_count = recurrent_query.shape[0]
    number_of_heads = recurrent_gate_lower_bound.shape[0] // HG_DK
    state_inflow, decay_logarithm = decay_factors(
        recurrent_forget_gate, recurrent_gate_lower_bound, recurrent_added_decay, number_of_heads
    )
    queries = recurrent_query.astype(jnp.float32).reshape(token_count, number_of_heads, HG_DK)
    value_rows = recurrent_value.astype(jnp.float32).reshape(token_count, number_of_heads, HG_DV)
    final_state, local_out = recurrence_blocks(
        queries, decay_logarithm, state_inflow, value_rows, BLK
    )
    running_log = jnp.cumsum(decay_logarithm, axis=0)
    through = jnp.exp(running_log[-1])
    incoming = carried_in(
        (through, final_state),
        "sp",
        chain_pair,
        (jnp.ones_like(through), jnp.zeros_like(final_state)),
    )
    carried = jnp.einsum(
        "thd,hdv->thv", queries * jnp.exp(running_log), incoming[1], precision=highest
    )
    return (
        head_norm(local_out + carried, recurrent_norm_gain)
        .astype(jnp.bfloat16)
        .reshape(token_count, -1)
    )


def attention_branch(
    attention_query_first,
    attention_key_first,
    attention_query_second,
    attention_key_second,
    attention_value,
    second_map_weight,
    attention_norm_gain,
):
    query_rows = attention_query_first.shape[0]
    key_heads = attention_key_first.shape[1] // DA_HD
    group_size = attention_query_first.shape[1] // DA_HD // key_heads
    score_scale = DA_HD ** (-0.5)
    offset = lax.axis_index("sp") * query_rows
    query_pos = offset + jnp.arange(query_rows)
    last_query = offset + query_rows - 1
    queries_one = attention_query_first.reshape(query_rows, key_heads, group_size, DA_HD)
    queries_two = attention_query_second.reshape(query_rows, key_heads, group_size, DA_HD)

    def map_update(running, queries, key_rows, value_rows, allowed):
        row_max, weight_mass, value_sum = running
        scores = (
            jnp.einsum("qkgd,skd->kgqs", queries, key_rows, preferred_element_type=jnp.float32)
            * score_scale
        )
        scores = jnp.where(allowed, scores, -1e30)
        new_max = jnp.maximum(row_max, jnp.max(scores, axis=-1))
        weights = jnp.where(allowed, jnp.exp(scores - new_max[..., None]), 0.0)
        shrink = jnp.exp(row_max - new_max)
        weight_mass = weight_mass * shrink + jnp.sum(weights, axis=-1)
        value_sum = value_sum * shrink[..., None] + jnp.einsum(
            "plew,wpd->pled",
            weights.astype(jnp.bfloat16),
            value_rows,
            preferred_element_type=jnp.float32,
        )
        return (new_max, weight_mass, value_sum)

    def key_block(running, block_one, block_two, block_values, first_row):
        span_rows = block_one.shape[0]
        key_pos = first_row + jnp.arange(span_rows)
        allowed = key_pos[None, :] <= query_pos[:, None]
        shaped_one = block_one.reshape(span_rows, key_heads, DA_HD)
        shaped_two = block_two.reshape(span_rows, key_heads, DA_HD)
        shaped_values = block_values.reshape(span_rows, key_heads, 2 * DA_HD)
        return (
            map_update(running[0], queries_one, shaped_one, shaped_values, allowed),
            map_update(running[1], queries_two, shaped_two, shaped_values, allowed),
        )

    def guarded_block(running, block_one, block_two, block_values, first_row):

        def compute(state_in):
            return key_block(state_in, block_one, block_two, block_values, first_row)

        def unchanged(state_in):
            return state_in

        result = lax.cond(first_row > last_query, unchanged, compute, running)
        return result

    start_max = jnp.full((key_heads, group_size, query_rows), -1e30, jnp.float32)
    zero_mass = jnp.zeros((key_heads, group_size, query_rows), jnp.float32)
    zero_sum = jnp.zeros((key_heads, group_size, query_rows, 2 * DA_HD), jnp.float32)
    fresh_state = (start_max, zero_mass, zero_sum)
    running = (fresh_state, fresh_state)
    shard_one = lax.all_gather(attention_key_first, "sp", axis=0, tiled=True)
    shard_two = lax.all_gather(attention_key_second, "sp", axis=0, tiled=True)
    shard_values = lax.all_gather(attention_value, "sp", axis=0, tiled=True)
    row_count = shard_one.shape[0]
    span_rows = min(row_count, key_span)
    full_count = row_count // span_rows

    def span_step(span_index, state_in):
        begin_row = span_index * span_rows
        return guarded_block(
            state_in,
            lax.dynamic_slice_in_dim(shard_one, begin_row, span_rows, 0),
            lax.dynamic_slice_in_dim(shard_two, begin_row, span_rows, 0),
            lax.dynamic_slice_in_dim(shard_values, begin_row, span_rows, 0),
            begin_row,
        )

    running = lax.fori_loop(0, full_count, span_step, running)
    first_map, second_map = running
    lambda_table = second_map_weight.reshape(key_heads, group_size)[:, :, None, None]
    combined = first_map[2] / first_map[1][..., None] - lambda_table * (
        second_map[2] / second_map[1][..., None]
    )
    combined = jnp.transpose(combined, (2, 0, 1, 3)).reshape(
        query_rows, key_heads * group_size, 2 * DA_HD
    )
    return head_norm(combined, attention_norm_gain).astype(jnp.bfloat16).reshape(query_rows, -1)


def shards(
    recurrent_query,
    recurrent_forget_gate,
    recurrent_value,
    recurrent_gate_lower_bound,
    recurrent_added_decay,
    recurrent_norm_gain,
    attention_query_first,
    attention_key_first,
    attention_query_second,
    attention_key_second,
    attention_value,
    second_map_weight,
    attention_norm_gain,
    output_weight,
):
    attended = attention_branch(
        attention_query_first,
        attention_key_first,
        attention_query_second,
        attention_key_second,
        attention_value,
        second_map_weight,
        attention_norm_gain,
    )
    recurrent_output = recurrent_path_output(
        recurrent_query,
        recurrent_forget_gate,
        recurrent_value,
        recurrent_gate_lower_bound,
        recurrent_added_decay,
        recurrent_norm_gain,
    )
    pieces = lax.all_gather(output_weight, "sp", axis=2, tiled=True)
    partial_terms = jnp.dot(
        recurrent_output, pieces[0], preferred_element_type=jnp.float32
    ) + jnp.dot(attended, pieces[1], preferred_element_type=jnp.float32)
    return lax.psum_scatter(
        partial_terms.astype(jnp.bfloat16), "tp", scatter_dimension=0, tiled=True
    )


def solution(mesh):
    return jax.shard_map(
        shards,
        mesh=mesh,
        in_specs=(
            P(("grp", "sp"), "tp"),
            P(("grp", "sp"), "tp"),
            P(("grp", "sp"), "tp"),
            P("tp"),
            P(("grp", "sp"), "tp"),
            P(),
            P(("grp", "sp"), "tp"),
            P(("grp", "sp"), "tp"),
            P(("grp", "sp"), "tp"),
            P(("grp", "sp"), "tp"),
            P(("grp", "sp"), "tp"),
            P("tp"),
            P(),
            P(None, "tp", "sp"),
        ),
        out_specs=P(("grp", "sp", "tp"), None),
        check_vma=False,
    )
```

profile of v0, /device:TPU:0, one launch (start us, length us, event | category | flops | bytes accessed | tf_op | source)
XLA Modules:
  0.0 149.0 jit_solution(5763729873363414824)
XLA Ops:
  6.5 0.7 all-gather.3.cloned.1.call-update
  7.3 0.7 divide_bitcast_fusion
  8.0 1.0 copy.151
  9.0 1.0 copy.148
  10.1 15.8 %all_gather.26 = bf16[1024,64]{0,1:T(8,128)(2,1)S(1)} all-gather(bf16[256,64]{0,1:T(8,128)(2,1)} %param.29), channel_id=1, replica_groups=mesh['grp'=2,'sp'=4,'tp'=4] {'sp'}, dimensions={0}, use_global_device_ids=true | all-gather | bytes 163840 | tf_op jit(solution)/shard_map/all_gather | solution.py:203
  25.9 0.8 copy.178
  28.4 16.7 %all_gather.27 = bf16[1024,128]{1,0:T(8,128)(2,1)S(1)} all-gather(bf16[256,128]{1,0:T(8,128)(2,1)S(1)} %copy-done.2), channel_id=1, replica_groups=mesh['grp'=2,'sp'=4,'tp'=4] {'sp'}, dimensions={0}, use_global_device_ids=true | all-gather | bytes 327680 | tf_op jit(solution)/shard_map/all_gather | solution.py:205
  45.1 0.5 log-plus-one_add_fusion
  45.6 24.4 %while.52 = (s32[]{:T(128)}, f32[2,128,128]{2,1,0:T(8,128)S(1)}, f32[8,32,2,128]{3,1,0,2:T(8,128)S(1)}, f32[8,32,2,128]{3,2,1,0:T(2,128)S(1)}, f32[8,32,2,128]{3...) while((s32[]{:T(128)}, f32[2,128,128]{2,1,0:T(8,128)S(1)}, ...), condition=%wide.region_2.3_spmd.clone, body=%wide.region_0.2_spmd.clone.sunk | while | flops 30302212 | bytes 3405956 | solution.py:84
  45.8 1.2 multiply_bitcast_fusion.2
  47.0 0.7 fusion.91
  48.2 0.4 convolution_add_fusion.3
  48.8 1.2 multiply_bitcast_fusion.2
  50.1 0.7 fusion.91
  51.3 0.4 convolution_add_fusion.3
  51.9 1.2 multiply_bitcast_fusion.2
  53.1 0.7 fusion.91
  54.3 0.4 convolution_add_fusion.3
  54.9 1.2 multiply_bitcast_fusion.2
  56.2 0.7 fusion.91
  57.4 0.4 convolution_add_fusion.3
  58.0 1.2 multiply_bitcast_fusion.2
  59.2 0.7 fusion.91
  60.4 0.4 convolution_add_fusion.3
  61.0 1.2 multiply_bitcast_fusion.2
  62.3 0.7 fusion.91
  63.5 0.4 convolution_add_fusion.3
  64.1 1.2 multiply_bitcast_fusion.2
  65.3 0.7 fusion.91
  66.5 0.4 convolution_add_fusion.3
  67.1 1.2 multiply_bitcast_fusion.2
  68.4 0.7 fusion.91
  69.6 0.4 convolution_add_fusion.3
  70.0 13.4 %all_gather.28 = bf16[1024,64]{0,1:T(8,128)(2,1)S(1)} all-gather(bf16[256,64]{0,1:T(8,128)(2,1)S(1)} %copy-done.5), channel_id=1, replica_groups=mesh['grp'=2,'sp'=4,'tp'=4] {'sp'}, dimensions={0}, use_global_device_ids=true | all-gather | bytes 163840 | tf_op jit(solution)/shard_map/all_gather | solution.py:204
  84.0 2.5 %while.51 = (s32[]{:T(128)}, f32[1,2,256]{2,1,0:T(2,128)S(1)}, f32[1,2,256]{2,1,0:T(2,128)S(1)}, f32[1,2,256,128]{3,2,1,0:T(8,128)S(1)}, f32[1,2,256]{2,1,0:T(2,...) while((s32[]{:T(128)}, f32[1,2,256]{2,1,0:T(2,128)S(1)}, ...), condition=%wide.region_15.16_spmd.clone, body=%wide.region_8.15_spmd.clone.sunk | while | flops 206442240 | bytes 8724921 | solution.py:220
  84.0 2.3 %conditional.3 = (f32[1,2,256]{2,1,0:T(2,128)S(1)}, f32[1,2,256]{2,1,0:T(2,128)S(1)}, f32[1,2,256,128]{3,2,1,0:T(8,128)S(1)}, f32[1,2,256]{2,1,0:T(2,128)S(1)}, ...) conditional(s32[]{:T(128)} %convert_element_type.97, (s32[]{:T(128)}, s32[]{:T(128)}, ...), branch_computations={%region_9.13_spmd, %region_14.14_spmd} | conditional | flops 206442240 | bytes 8715370 | solution.py:195
  84.2 0.3 fusion.69
  84.6 0.5 fusion.9
  85.1 0.3 fusion.68
  85.4 0.4 fusion.13
  85.8 0.5 fusion.8
  86.9 13.0 %all_gather.22 = bf16[4,2,128]{2,1,0:T(2,128)(2,1)S(1)} all-gather(bf16[1,2,128]{2,1,0:T(2,128)(2,1)S(1)} %fusion.67), channel_id=1, replica_groups=mesh['grp'=2,'sp'=4,'tp'=4] {'sp'}, dimensions={0}, use_global_device_ids=true | all-gather | bytes 2560 | tf_op jit(solution)/shard_map/all_gather | solution.py:18
  99.9 13.8 %all-gather = bf16[8,128,128]{2,1,0:T(8,128)(2,1)S(1)} all-gather(bf16[2,128,128]{2,1,0:T(8,128)(2,1)S(1)} %convert_element_type.73), channel_id=2, replica_groups=mesh['grp'=2,'sp'=4,'tp'=4] {'sp'}, dimensions={0}, use_global_device_ids=true | all-gather | bytes 327680 | tf_op jit(solution)/shard_map/all_gather | solution.py:18
  114.2 0.7 while.53
  114.9 0.4 multiply_reduce_fusion
  115.6 1.8 %fusion.60 = f32[256,2048]{1,0:T(8,128)S(1)} fusion(bf16[256,256]{0,1:T(8,128)(2,1)S(1)} %bitcast.210, bf16[2,256,2048]{2,1,0:T(8,128)(2,1)} %all-gather.3.cloned.1.call-done), kind=kOutput, calls=%fused_computation.91 | convolution fusion | flops 268435456 | bytes 3276800 | tf_op jit(solution)/shard_map/dot_general | solution.py:266
  117.5 1.4 fusion.58
  119.0 23.2 %reduce-scatter.2.cloned.1.call-done = bf16[64,2048]{1,0:T(8,128)(2,1)} async-done(((bf16[256,2048]{1,0:T(8,128)(2,1)}), bf16[64,2048]{1,0:T(8,128)(2,1)}) %reduce-scatter.2.cloned.1.call-update) | async-done | bytes 262160 | tf_op jit(solution)/shard_map/reduce_scatter | solution.py:269
  (174 shorter events, 8.9 us)
Async XLA Ops:
  6.5 20.3 %copy-start.6 = (f32[256,2]{0,1:T(2,128)S(1)}, f32[256,2]{0,1:T(2,128)}, u32[]{:S(2)}) copy-start(f32[256,2]{0,1:T(2,128)} %param.26) | copy-start | bytes 6148
  6.5 109.0 %all-gather.3.cloned.1.call-start = ((), (), s32[]{:S(2)}) async-start(), calls=%async_computation.1 | async-start | bytes 2621440 | tf_op jit(solution)/shard_map/all_gather | solution.py:265
  7.3 134.9 %reduce-scatter.2.cloned.1.call-start = ((), (), s32[]{:S(2)}) async-start(), calls=%async_computation.2 | async-start | bytes 1310720 | tf_op jit(solution)/shard_map/reduce_scatter | solution.py:269
  27.1 1.2 copy-start.1
  27.2 1.2 copy-start.2
  45.5 24.5 %copy-start.5 = (bf16[256,64]{0,1:T(8,128)(2,1)S(1)}, bf16[256,64]{0,1:T(8,128)(2,1)}, u32[]{:S(2)}) copy-start(bf16[256,64]{0,1:T(8,128)(2,1)} %param.31) | copy-start | bytes 98308
  45.5 37.9 %copy-start.3 = (bf16[256,128]{1,0:T(8,128)(2,1)S(1)}, bf16[256,128]{1,0:T(8,128)(2,1)}, u32[]{:S(2)}) copy-start(bf16[256,128]{1,0:T(8,128)(2,1)} %param.28) | copy-start | bytes 196612
  45.6 38.0 %copy-start.4 = (bf16[256,128]{1,0:T(8,128)(2,1)S(1)}, bf16[256,128]{1,0:T(8,128)(2,1)}, u32[]{:S(2)}) copy-start(bf16[256,128]{1,0:T(8,128)(2,1)} %param.30) | copy-start | bytes 196612
  86.5 27.2 %copy-start.9 = (f32[2]{0:T(128)S(1)}, f32[2]{0:T(128)}, u32[]{:S(2)}) copy-start(f32[2]{0:T(128)} %param.33) | copy-start | bytes 28
  113.7 1.6 %copy-start.7 = (f32[128]{0:T(128)S(1)}, f32[128]{0:T(128)}, u32[]{:S(2)}) copy-start(f32[128]{0:T(128)} %param.34) | copy-start | bytes 1540
  113.8 1.6 %copy-start.8 = (f32[128]{0:T(128)S(1)}, f32[128]{0:T(128)}, u32[]{:S(2)}) copy-start(f32[128]{0:T(128)} %param.27) | copy-start | bytes 1540
  115.6 1.9 %copy-start = (bf16[2,256,2048]{2,1,0:T(8,128)(2,1)S(1)}, bf16[2,256,2048]{2,1,0:T(8,128)(2,1)}, u32[]{:S(2)}) copy-start(bf16[2,256,2048]{2,1,0:T(8,128)(2,1)} %all-gather.3.cloned.1.call-done) | copy-start | bytes 6291460
Sparse Core Ops, SparseCore 0:
  8.9 53.0 all-gather.2
  119.1 23.0 reduce-scatter.1
where the time goes:
time: 149 us
  blocking collectives  72.7 us (49%)
  waiting for transfers between devices  24 us (16%)
  other arithmetic  19.9 us (13%)
  between operations  13.9 us (9%)
  matrix products  12.3 us (8%)
  local copies, waits for them, and re-layouts  5.09 us (3%)
    all_gather x2, blocking collectives, carried_in(): lax.all_gather(part.astype(kind), axis)  26.8 us
    reduce_scatter x1, waiting for transfers between devices, shards(): lax.psum_scatter(partial_terms.astype(jnp.bfloat16), 'tp', scatter_dimens...  23.2 us
    all_gather x1, blocking collectives, attention_branch(): shard_values = lax.all_gather(attention_value, 'sp', axis=0, tiled=True)  16.7 us
    all_gather x1, blocking collectives, attention_branch(): shard_one = lax.all_gather(attention_key_first, 'sp', axis=0, tiled=True)  15.8 us
    all_gather x1, blocking collectives, attention_branch(): shard_two = lax.all_gather(attention_key_second, 'sp', axis=0, tiled=True)  13.4 us
    while x8, other arithmetic  9.95 us
    dot_general x8, other arithmetic, block_step(): jnp.einsum('thd,shd,tshd->hts', query_blk, inflow_blk, decay_table, preci...  5.65 us
    dot_general x8, matrix products, block_step(): jnp.einsum('shd,shv->hdv', inflow_blk * jnp.exp(last_log[None] - cumulati...  3.16 us
  transfers between devices with their start and end apart: 2, of which 1 were waited for; matrix products, arithmetic and copies ran while one was open for 23% of the time, Pallas kernels for 0%

commit v1 on v0

--- a/solution.py
+++ b/solution.py
@@ -1,3 +1,4 @@
+import functools
 import jax
 import jax.numpy as jnp
 from jax import lax
@@ -10,6 +11,25 @@
 epsilon = 1e-06
 highest = lax.Precision.HIGHEST
 key_span = 512
+
+
+def cut_the_view(x_part, group_axis):
+    shelf = []
+    it = 0
+    chips = lax.axis_size(group_axis)
+    while it < chips:
+        shelf.append((it, (it + 1) % chips))
+        it = it + 1
+    vec_out = [None] * chips
+    vec_out[chips - 1] = x_part
+    for rr in range(chips - 2, -1, -1):
+        vec_out[rr] = lax.ppermute(vec_out[rr + 1], group_axis, shelf)
+    return jnp.roll(
+        jnp.concatenate(vec_out, 0), (lax.axis_index(group_axis) + 1) * x_part.shape[0], 0
+    )
+
+
+take_slots = functools.partial(cut_the_view, group_axis="sp")
 
 
 def carried_in(array, axis, combine, identity):
@@ -200,7 +220,7 @@
     zero_sum = jnp.zeros((key_heads, group_size, query_rows, 2 * DA_HD), jnp.float32)
     fresh_state = (start_max, zero_mass, zero_sum)
     running = (fresh_state, fresh_state)
-    shard_one = lax.all_gather(attention_key_first, "sp", axis=0, tiled=True)
+    shard_one = take_slots(attention_key_first)
     shard_two = lax.all_gather(attention_key_second, "sp", axis=0, tiled=True)
     shard_values = lax.all_gather(attention_value, "sp", axis=0, tiled=True)
     row_count = shard_one.shape[0]

time: 149 us -> 137 us (0.919)
  blocking collectives: 72.7 us -> 54.9 us
  starting transfers between devices: 0.04 us -> 5.09 us
  waiting for transfers between devices: 24 us -> 26.9 us
  local copies, waits for them, and re-layouts: 5.09 us -> 3.52 us
    all_gather x1 -> x0, blocking collectives: 15.8 us -> none  [attention_branch(): shard_one = lax.all_gather(attention_key_first, 'sp', axis=0, tiled=True)]
    ppermute x0 -> x3, starting transfers between devices: none -> 5.01 us  [cut_the_view(): vec_out[rr] = lax.ppermute(vec_out[rr + 1], group_axis, shelf)]
    reduce_scatter x1, waiting for transfers between devices: 23.2 us -> 26.8 us  [shards(): lax.psum_scatter(partial_terms.astype(jnp.bfloat16), 'tp', scatter_dimens...]
    all_gather x1, blocking collectives: 16.7 us -> 14.5 us  [attention_branch(): shard_values = lax.all_gather(attention_value, 'sp', axis=0, tiled=True)]
  transfers between devices with their start and end apart: 2 -> 5, of which waited for: 1 -> 1; matrix products, arithmetic and copies ran while one was open for 23% -> 23% of each run, Pallas kernels for 0% -> 0%
where the time goes in v1:
time: 137 us
  blocking collectives  54.9 us (40%)
  waiting for transfers between devices  26.9 us (20%)
  other arithmetic  19.2 us (14%)
  between operations  14 us (10%)
  matrix products  12.3 us (9%)
  starting transfers between devices  5.09 us (4%)
  local copies, waits for them, and re-layouts  3.52 us (3%)
    all_gather x2, blocking collectives, carried_in(): lax.all_gather(part.astype(kind), axis)  26.9 us
    reduce_scatter x1, waiting for transfers between devices, shards(): lax.psum_scatter(partial_terms.astype(jnp.bfloat16), 'tp', scatter_dimens...  26.8 us
    all_gather x1, blocking collectives, attention_branch(): shard_values = lax.all_gather(attention_value, 'sp', axis=0, tiled=True)  14.5 us
    all_gather x1, blocking collectives, attention_branch(): shard_two = lax.all_gather(attention_key_second, 'sp', axis=0, tiled=True)  13.5 us
    while x8, other arithmetic  9.95 us
    dot_general x8, other arithmetic, block_step(): jnp.einsum('thd,shd,tshd->hts', query_blk, inflow_blk, decay_table, preci...  5.65 us
    ppermute x3, starting transfers between devices, cut_the_view(): vec_out[rr] = lax.ppermute(vec_out[rr + 1], group_axis, shelf)  5.01 us
    dot_general x8, matrix products, block_step(): jnp.einsum('shd,shv->hdv', inflow_blk * jnp.exp(last_log[None] - cumulati...  3.15 us
  transfers between devices with their start and end apart: 5, of which 1 were waited for; matrix products, arithmetic and copies ran while one was open for 23% of the time, Pallas kernels for 0%

profile of v1, /device:TPU:0, one launch (start us, length us, event | category | flops | bytes accessed | tf_op | source)
XLA Modules:
  0.0 137.0 jit_solution(8199558663500702932)
XLA Ops:
  6.6 3.1 %collective-permute-start = (bf16[256,64]{0,1:T(8,128)(2,1)}, bf16[256,64]{0,1:T(8,128)(2,1)S(1)}, u32[]{:S(2)}, u32[]{:S(2)}) collective-permute-start(bf16[256,64]{0,1:T(8,128)(2,1)} %param.29), channel_id=1, source_target_pairs={{0,4},{4,8},{8,12},{12,0},{1,5},{5,9},{9,13},{13,1},{2,6},{6,10},{... | collective-permute-start | bytes 98312 | tf_op jit(solution)/shard_map/ppermute | solution.py:26
  9.8 1.0 copy.148
  11.9 0.5 log-plus-one_add_fusion
  12.3 24.4 %while.52 = (s32[]{:T(128)}, f32[2,128,128]{2,1,0:T(8,128)S(1)}, f32[8,32,2,128]{3,1,0,2:T(8,128)S(1)}, f32[8,32,2,128]{3,2,1,0:T(2,128)S(1)}, f32[8,32,2,128]{3...) while((s32[]{:T(128)}, f32[2,128,128]{2,1,0:T(8,128)S(1)}, ...), condition=%wide.region_2.3_spmd.clone, body=%wide.region_0.2_spmd.clone.sunk | while | flops 30302212 | bytes 3405948 | solution.py:104
  12.4 1.2 multiply_bitcast_fusion.2
  13.7 0.7 fusion.91
  14.4 0.2 convolution_bitcast_fusion.6
  14.7 0.2 fusion.92
  15.0 0.4 convolution_add_fusion.3
  15.5 1.2 multiply_bitcast_fusion.2
  16.7 0.7 fusion.91
  18.0 0.4 convolution_add_fusion.3
  18.5 1.2 multiply_bitcast_fusion.2
  19.8 0.7 fusion.91
  21.1 0.4 convolution_add_fusion.3
  21.6 1.2 multiply_bitcast_fusion.2
  22.8 0.7 fusion.91
  24.1 0.4 convolution_add_fusion.3
  24.6 1.2 multiply_bitcast_fusion.2
  25.9 0.7 fusion.91
  27.2 0.4 convolution_add_fusion.3
  27.7 1.2 multiply_bitcast_fusion.2
  28.9 0.7 fusion.91
  30.2 0.4 convolution_add_fusion.3
  30.7 1.2 multiply_bitcast_fusion.2
  32.0 0.7 fusion.91
  33.3 0.4 convolution_add_fusion.3
  33.8 1.2 multiply_bitcast_fusion.2
  35.0 0.7 fusion.91
  36.3 0.4 convolution_add_fusion.3
  36.7 16.3 %all-gather = bf16[8,128,128]{2,1,0:T(8,128)(2,1)S(1)} all-gather(bf16[2,128,128]{2,1,0:T(8,128)(2,1)S(1)} %convert_element_type.73), channel_id=2, replica_groups=mesh['grp'=2,'sp'=4,'tp'=4] {'sp'}, dimensions={0}, use_global_device_ids=true | all-gather | bytes 327680 | tf_op jit(solution)/shard_map/all_gather | solution.py:38
  54.0 10.6 %all_gather.19 = bf16[4,2,128]{2,1,0:T(2,128)(2,1)S(1)} all-gather(bf16[1,2,128]{2,1,0:T(2,128)(2,1)S(1)} %fusion.67), channel_id=1, replica_groups=mesh['grp'=2,'sp'=4,'tp'=4] {'sp'}, dimensions={0}, use_global_device_ids=true | all-gather | bytes 2560 | tf_op jit(solution)/shard_map/all_gather | solution.py:38
  64.6 0.7 while.53
  65.6 0.3 exponential_multiply_fusion
  65.9 0.4 multiply_reduce_fusion
  66.6 14.5 %all_gather.23 = bf16[1024,128]{1,0:T(8,128)(2,1)S(1)} all-gather(bf16[256,128]{1,0:T(8,128)(2,1)S(1)} %copy-done.4), channel_id=1, replica_groups=mesh['grp'=2,'sp'=4,'tp'=4] {'sp'}, dimensions={0}, use_global_device_ids=true | all-gather | bytes 327680 | tf_op jit(solution)/shard_map/all_gather | solution.py:225
  81.3 1.8 %collective-permute-start.2 = (bf16[256,64]{0,1:T(8,128)(2,1)S(1)}, bf16[256,64]{0,1:T(8,128)(2,1)S(1)}, u32[]{:S(2)}, u32[]{:S(2)}) collective-permute-start(bf16[256,64]{0,1:T(8,128)(2,1)S(1)} %collective-permute-done.1), channel_id=1, source_target_pairs={{0,4},{4,8},{8,12},{12,0},{1,5},{5,9},{9,13},{13,1},{2,6},{6,10},{... | collective-permute-start | bytes 98312 | tf_op jit(solution)/shard_map/ppermute | solution.py:26
  83.2 13.5 %all_gather.24 = bf16[1024,64]{0,1:T(8,128)(2,1)S(1)} all-gather(bf16[256,64]{0,1:T(8,128)(2,1)S(1)} %copy-done.7), channel_id=1, replica_groups=mesh['grp'=2,'sp'=4,'tp'=4] {'sp'}, dimensions={0}, use_global_device_ids=true | all-gather | bytes 163840 | tf_op jit(solution)/shard_map/all_gather | solution.py:224
  96.9 2.5 %while.51 = (s32[]{:T(128)}, f32[1,2,256]{2,1,0:T(2,128)S(1)}, f32[1,2,256]{2,1,0:T(2,128)S(1)}, f32[1,2,256,128]{3,2,1,0:T(8,128)S(1)}, f32[1,2,256]{2,1,0:T(2,...) while((s32[]{:T(128)}, f32[1,2,256]{2,1,0:T(2,128)S(1)}, ...), condition=%wide.region_15.16_spmd.clone, body=%wide.region_8.15_spmd.clone.sunk | while | flops 206442240 | bytes 8724921 | solution.py:240
  96.9 2.3 %conditional.3 = (f32[1,2,256]{2,1,0:T(2,128)S(1)}, f32[1,2,256]{2,1,0:T(2,128)S(1)}, f32[1,2,256,128]{3,2,1,0:T(8,128)S(1)}, f32[1,2,256]{2,1,0:T(2,128)S(1)}, ...) conditional(s32[]{:T(128)} %convert_element_type.97, (s32[]{:T(128)}, s32[]{:T(128)}, ...), branch_computations={%region_9.13_spmd, %region_14.14_spmd} | conditional | flops 206442240 | bytes 8715370 | solution.py:215
  97.1 0.3 fusion.69
  97.5 0.5 fusion.9
  98.0 0.3 fusion.68
  98.3 0.5 fusion.8
  98.8 0.4 fusion.13
  100.0 1.8 %fusion.60 = f32[256,2048]{1,0:T(8,128)S(1)} fusion(bf16[256,256]{0,1:T(8,128)(2,1)S(1)} %bitcast.209, bf16[2,256,2048]{2,1,0:T(8,128)(2,1)} %all-gather.3.cloned.1.call-done), kind=kOutput, calls=%fused_computation.91 | convolution fusion | flops 268435456 | bytes 3276800 | tf_op jit(solution)/shard_map/dot_general | solution.py:286
  101.9 1.4 %fusion.58 = bf16[256,2048]{1,0:T(8,128)(2,1)} fusion(f32[256,2048]{1,0:T(8,128)S(1)} %fusion.60, bf16[256,256]{0,1:T(8,128)(2,1)S(1)} %bitcast.210, bf16[2,256,2048]{2,1,0:T(8,128)(2,1)S(1)} %copy-done), kind=kOutput, calls=%fused_computation.86 | convolution fusion | flops 269484032 | bytes 4325376 | tf_op jit(solution)/shard_map/dot_general | solution.py:288
  103.3 26.8 %reduce-scatter.2.cloned.1.call-done = bf16[64,2048]{1,0:T(8,128)(2,1)} async-done(((bf16[256,2048]{1,0:T(8,128)(2,1)}), bf16[64,2048]{1,0:T(8,128)(2,1)}) %reduce-scatter.2.cloned.1.call-update) | async-done | bytes 262160 | tf_op jit(solution)/shard_map/reduce_scatter | solution.py:289
  (194 shorter events, 8.5 us)
Async XLA Ops:
  6.5 4.6 %copy-start.9 = (f32[256]{0:T(256)S(1)}, f32[256]{0:T(256)}, u32[]{:S(2)}) copy-start(f32[256]{0:T(256)} %param.25) | copy-start | bytes 3076
  6.5 4.7 %copy-start.8 = (f32[256,2]{0,1:T(2,128)S(1)}, f32[256,2]{0,1:T(2,128)}, u32[]{:S(2)}) copy-start(f32[256,2]{0,1:T(2,128)} %param.26) | copy-start | bytes 6148
  6.5 4.8 %copy-start.2 = (bf16[256,256]{1,0:T(8,128)(2,1)S(1)}, bf16[256,256]{1,0:T(8,128)(2,1)}, u32[]{:S(2)}) copy-start(bf16[256,256]{1,0:T(8,128)(2,1)} %param.22) | copy-start | bytes 393220
  6.5 5.2 %copy-start.1 = (bf16[256,256]{1,0:T(8,128)(2,1)S(1)}, bf16[256,256]{1,0:T(8,128)(2,1)}, u32[]{:S(2)}) copy-start(bf16[256,256]{1,0:T(8,128)(2,1)} %param.24) | copy-start | bytes 393220
  6.5 93.4 %all-gather.3.cloned.1.call-start = ((), (), s32[]{:S(2)}) async-start(), calls=%async_computation.1 | async-start | bytes 2621440 | tf_op jit(solution)/shard_map/all_gather | solution.py:285
  6.6 59.9 %collective-permute-start = (bf16[256,64]{0,1:T(8,128)(2,1)}, bf16[256,64]{0,1:T(8,128)(2,1)S(1)}, u32[]{:S(2)}, u32[]{:S(2)}) collective-permute-start(bf16[256,64]{0,1:T(8,128)(2,1)} %param.29), channel_id=1, source_target_pairs={{0,4},{4,8},{8,12},{12,0},{1,5},{5,9},{9,13},{13,1},{2,6},{6,10},{... | collective-permute-start | bytes 98312 | tf_op jit(solution)/shard_map/ppermute | solution.py:26
  9.7 120.4 %reduce-scatter.2.cloned.1.call-start = ((), (), s32[]{:S(2)}) async-start(), calls=%async_computation.2 | async-start | bytes 1310720 | tf_op jit(solution)/shard_map/reduce_scatter | solution.py:289
  64.6 1.8 %copy-start.10 = (f32[128]{0:T(128)S(1)}, f32[128]{0:T(128)}, u32[]{:S(2)}) copy-start(f32[128]{0:T(128)} %param.27) | copy-start | bytes 1540
  65.2 1.3 copy-start.4
  65.2 15.8 %copy-start.5 = (bf16[256,128]{1,0:T(8,128)(2,1)S(1)}, bf16[256,128]{1,0:T(8,128)(2,1)}, u32[]{:S(2)}) copy-start(bf16[256,128]{1,0:T(8,128)(2,1)} %param.28) | copy-start | bytes 196612
  65.3 15.9 %copy-start.6 = (bf16[256,128]{1,0:T(8,128)(2,1)S(1)}, bf16[256,128]{1,0:T(8,128)(2,1)}, u32[]{:S(2)}) copy-start(bf16[256,128]{1,0:T(8,128)(2,1)} %param.30) | copy-start | bytes 196612
  65.3 17.9 %copy-start.7 = (bf16[256,64]{0,1:T(8,128)(2,1)S(1)}, bf16[256,64]{0,1:T(8,128)(2,1)}, u32[]{:S(2)}) copy-start(bf16[256,64]{0,1:T(8,128)(2,1)} %param.31) | copy-start | bytes 98308
  65.3 31.4 %copy-start.3 = (bf16[256,64]{0,1:T(8,128)(2,1)S(1)}, bf16[256,64]{0,1:T(8,128)(2,1)}, u32[]{:S(2)}) copy-start(bf16[256,64]{0,1:T(8,128)(2,1)} %param.29) | copy-start | bytes 98308
  66.5 14.9 %collective-permute-start.1 = (bf16[256,64]{0,1:T(8,128)(2,1)S(1)}, bf16[256,64]{0,1:T(8,128)(2,1)S(1)}, u32[]{:S(2)}, u32[]{:S(2)}) collective-permute-start(bf16[256,64]{0,1:T(8,128)(2,1)S(1)} %collective-permute-done), channel_id=1, source_target_pairs={{0,4},{4,8},{8,12},{12,0},{1,5},{5,9},{9,13},{13,1},{2,6},{6,10},{... | collective-permute-start | bytes 98312 | tf_op jit(solution)/shard_map/ppermute | solution.py:26
  81.3 15.3 %collective-permute-start.2 = (bf16[256,64]{0,1:T(8,128)(2,1)S(1)}, bf16[256,64]{0,1:T(8,128)(2,1)S(1)}, u32[]{:S(2)}, u32[]{:S(2)}) collective-permute-start(bf16[256,64]{0,1:T(8,128)(2,1)S(1)} %collective-permute-done.1), channel_id=1, source_target_pairs={{0,4},{4,8},{8,12},{12,0},{1,5},{5,9},{9,13},{13,1},{2,6},{6,10},{... | collective-permute-start | bytes 98312 | tf_op jit(solution)/shard_map/ppermute | solution.py:26
  96.9 2.8 %copy-start.12 = (f32[2]{0:T(128)S(1)}, f32[2]{0:T(128)}, u32[]{:S(2)}) copy-start(f32[2]{0:T(128)} %param.33) | copy-start | bytes 28
  96.9 2.9 %copy-start.11 = (f32[128]{0:T(128)S(1)}, f32[128]{0:T(128)}, u32[]{:S(2)}) copy-start(f32[128]{0:T(128)} %param.34) | copy-start | bytes 1540
  99.9 1.9 %copy-start = (bf16[2,256,2048]{2,1,0:T(8,128)(2,1)S(1)}, bf16[2,256,2048]{2,1,0:T(8,128)(2,1)}, u32[]{:S(2)}) copy-start(bf16[2,256,2048]{2,1,0:T(8,128)(2,1)} %all-gather.3.cloned.1.call-done) | copy-start | bytes 6291460
Sparse Core Ops, SparseCore 0:
  9.8 51.6 all-gather.2
  103.4 26.6 reduce-scatter.1
